TPU v7x, 512 devices: a whole 4x4x16 slice. The times are simulated.
512 devices in a mesh: fs: 64 (over z, y), tp: 8 (over x, core).
Axes of the slice: x: 4, y: 4, z: 16, core: 2. Of those that a mesh axis runs over, the one named last changes fastest.
Arguments:
- tokens: bfloat16 [16384, 2048], P('fs'), may hold values from -6 to 6
- recurrent_input_gain: bfloat16 [2048], replicated, may hold values from 0.099609375 to 1.8984375
- recurrent_branch_weight: bfloat16 [2048, 1024], P('fs', 'tp'), may hold values from -0.125 to 0.125
- output_gate_weight: bfloat16 [2048, 1024], P('fs', 'tp'), may hold values from -0.125 to 0.125
- filter_taps: bfloat16 [4, 1024], P(None, 'tp'), may hold values from -3 to 3
- retention_gate_blocks: bfloat16 [2, 8, 128, 128], P(None, 'tp'), may hold values from -0.5 to 0.5
- input_gate_blocks: bfloat16 [2, 8, 128, 128], P(None, 'tp'), may hold values from -0.5 to 0.5
- channel_decay_rate: float32 [2, 1024], P(None, 'tp'), may hold values from 0 to 0.008, as said below
- position_log_decay: float32 [2, 16384, 1024], P(None, 'fs', 'tp'), may hold values from -0.7 to 0, as said below
- recurrent_output_weight: bfloat16 [1024, 2048], P('tp', 'fs'), may hold values from -0.1875 to 0.1875
- recurrent_output_gain: bfloat16 [2048], replicated, may hold values from 0.099609375 to 1.8984375
- feedforward_norm_gain: bfloat16 [2048], replicated, may hold values from 0.099609375 to 1.8984375
- feedforward_up_weight: bfloat16 [2048, 8192], P('fs', 'tp'), may hold values from -0.125 to 0.125
- feedforward_down_weight: bfloat16 [8192, 2048], P('tp', 'fs'), may hold values from -0.0625 to 0.0625
- feedforward_output_gain: bfloat16 [2048], replicated, may hold values from 0.099609375 to 1.8984375
Outputs:
- layer_out: bfloat16 [16384, 2048], P('fs')
Inputs may be any that keep to these rules, and one draw needn't show every extreme that they name: `channel_decay_rate`: positive rates, one for each channel and direction. `position_log_decay`: zero except at a few positions of each sequence and channel.
All inputs are finite; a program needn't handle non-finite values.
Results may differ from a plain program's by a relative error of at most 0.02.
Values may be sent and summed in bfloat16 or wider, within the bound.
No kernel may reach another device: no remote copies, remote signals or barrier semaphores. Data moves between devices by JAX's collectives and lax.ppermute only.
A program may use at most 128 MiB of HBM per device.

v0:
```python
import jax
import jax.numpy as jnp
from jax import lax
from jax.sharding import Mesh
from jax.sharding import PartitionSpec as P

FS = ("fs_0", "fs_1")


EPS = 1e-06
GATE_STEEPNESS = 8.0


def sent_together(arrays, axis, dim, along):
    ends, at = ([], 0)
    for a in arrays[:-1]:
        at += a.shape[along]
        ends.append(at)
    both = jnp.concatenate(arrays, axis=along)
    return tuple(jnp.split(lax.all_gather(both, axis, axis=dim, tiled=True), ends, axis=along))


def gathered_by_axis(array, axes, dim):
    out = array
    for number in range(len(axes) - 1, -1, -1):
        out = lax.all_gather(out, axes[number], axis=dim, tiled=True)
    return out


def from_everyone(array, axis):
    copies = jnp.broadcast_to(array, (lax.axis_size(axis), *array.shape))
    return lax.all_to_all(copies, axis, split_axis=0, concat_axis=0, tiled=True)


def taken_together(array, axis):
    everything = from_everyone(array, axis)
    return jnp.sum(everything.astype(jnp.float32), axis=0)


def root_norm(values, gain):
    return (
        values
        * lax.rsqrt(jnp.mean(values * values, axis=-1, keepdims=True) + EPS)
        * gain.astype(jnp.float32)
    )


def combine(earlier, later):
    return (earlier[0] * later[0], later[0] * earlier[1] + later[1])


def centred_conv(signal, taps):
    length = signal.shape[0]
    width_taps = taps.shape[0]
    left_pad = width_taps // 2
    padded = jnp.pad(signal.astype(jnp.float32), ((left_pad, width_taps - 1 - left_pad), (0, 0)))
    total = jnp.zeros(signal.shape, jnp.float32)
    for offset in range(width_taps):
        total = total + padded[offset : offset + length] * taps[offset].astype(jnp.float32)
    return total.astype(jnp.bfloat16)


def block_map(signal, matrices):
    block_width = matrices.shape[-1]
    shaped = signal.reshape(signal.shape[0], matrices.shape[0], block_width)
    mapped = jnp.einsum("tnc,ncd->tnd", shaped, matrices, preferred_element_type=jnp.float32)
    return mapped.reshape(signal.shape)


def linear_recurrence(
    convolved_output,
    retention_matrices,
    input_gate_matrices,
    decay_rate_row,
    decay_extra_block,
    reversed_scan,
):
    retention_gate = jax.nn.sigmoid(block_map(convolved_output, retention_matrices))
    admit = jax.nn.sigmoid(block_map(convolved_output, input_gate_matrices))
    logarithm_decay = -GATE_STEEPNESS * retention_gate * decay_rate_row[None, :] + decay_extra_block
    decay = jnp.exp(logarithm_decay)
    drive = jnp.sqrt(-jnp.expm1(2.0 * logarithm_decay)) * (
        admit * convolved_output.astype(jnp.float32)
    )
    _, state = lax.associative_scan(combine, (decay, drive), reverse=reversed_scan, axis=0)
    return state


def per_device(
    tokens,
    recurrent_input_gain,
    recurrent_branch_weight,
    output_gate_weight,
    filter_taps,
    retention_gate_blocks,
    input_gate_blocks,
    channel_decay_rate,
    position_log_decay,
    recurrent_output_weight,
    recurrent_output_gain,
    feedforward_norm_gain,
    feedforward_up_weight,
    feedforward_down_weight,
    feedforward_output_gain,
):
    normed = root_norm(tokens.astype(jnp.float32), recurrent_input_gain).astype(jnp.bfloat16)
    pieces = sent_together((recurrent_branch_weight, output_gate_weight), FS, 0, 1)
    columns = normed
    recur_sum = jnp.dot(columns, pieces[0], preferred_element_type=jnp.float32)
    gate_sum = jnp.dot(columns, pieces[1], preferred_element_type=jnp.float32)
    recur_in = recur_sum.astype(jnp.bfloat16)
    gate_in = lax.optimization_barrier(gate_sum.astype(jnp.bfloat16))
    convolved_output = lax.optimization_barrier(centred_conv(recur_in, filter_taps))
    forward_sweep = linear_recurrence(
        convolved_output,
        retention_gate_blocks[0],
        input_gate_blocks[0],
        channel_decay_rate[0],
        position_log_decay[0],
        False,
    )
    backward_sweep = linear_recurrence(
        convolved_output,
        retention_gate_blocks[1],
        input_gate_blocks[1],
        channel_decay_rate[1],
        position_log_decay[1],
        True,
    )
    hidden = ((forward_sweep + backward_sweep) * jax.nn.gelu(gate_in.astype(jnp.float32))).astype(
        jnp.bfloat16
    )
    mixer_cols = gathered_by_axis(recurrent_output_weight, FS, 1)
    partial_value = jnp.dot(hidden, mixer_cols, preferred_element_type=jnp.float32)
    mixed = taken_together(partial_value.astype(jnp.bfloat16), "tp").astype(jnp.float32)
    stream = lax.optimization_barrier(
        (tokens.astype(jnp.float32) + root_norm(mixed, recurrent_output_gain)).astype(jnp.bfloat16)
    )
    normed_ff = root_norm(stream.astype(jnp.float32), feedforward_norm_gain).astype(jnp.bfloat16)
    columns = normed_ff
    lifted_sum = jnp.dot(
        columns, gathered_by_axis(feedforward_up_weight, FS, 0), preferred_element_type=jnp.float32
    )
    lifted = jnp.square(jax.nn.relu(lifted_sum)).astype(jnp.bfloat16)
    down_cols = gathered_by_axis(feedforward_down_weight, FS, 1)
    lowered_part = jnp.dot(lifted, down_cols, preferred_element_type=jnp.float32)
    lowered = taken_together(lowered_part.astype(jnp.bfloat16), "tp").astype(jnp.float32)
    return (stream.astype(jnp.float32) + root_norm(lowered, feedforward_output_gain)).astype(
        jnp.bfloat16
    )


def solution(mesh):
    split = Mesh(mesh.devices.reshape(16, 4, mesh.shape["tp"]), ("fs_0", "fs_1", "tp"))
    placed = (
        P(FS, None),
        P(),
        P(FS, "tp"),
        P(FS, "tp"),
        P(None, "tp"),
        P(None, "tp", None, None),
        P(None, "tp", None, None),
        P(None, "tp"),
        P(None, FS, "tp"),
        P("tp", FS),
        P(),
        P(),
        P(FS, "tp"),
        P("tp", FS),
        P(),
    )
    return jax.shard_map(
        per_device, mesh=split, in_specs=placed, out_specs=P(FS, None), check_vma=False
    )
```

profile of v0, /device:TPU:1, one launch (start us, length us, event | category | flops | bytes accessed | tf_op | source)
XLA Modules:
  0.0 431.3 jit_solution(9742989788884283247)
XLA Ops:
  6.5 1.4 pad_maximum_fusion.4
  8.0 12.7 %all_gather.24 = bf16[128,1024]{1,0:T(8,128)(2,1)} all-gather(bf16[32,1024]{1,0:T(8,128)(2,1)} %param.27), channel_id=1, replica_groups=mesh['fs_0'=16,'fs_1'=4,'tp'=8] {'fs_1'}, dimensions={0}, use_global_device_ids=true | all-gather | bytes 327680 | tf_op jit(solution)/shard_map/all_gather | solution.py:26
  20.7 0.7 convert_element_type.80
  21.4 1.6 fusion
  23.0 0.8 bitcast_convert_fusion.3
  23.8 0.8 multiply_bitcast_fusion.1
  24.6 9.2 %all_gather.22 = bf16[128,128]{0,1:T(8,128)(2,1)S(1)} all-gather(bf16[128,32]{0,1:T(8,128)(2,1)} %param.24), channel_id=1, replica_groups=mesh['fs_0'=16,'fs_1'=4,'tp'=8] {'fs_1'}, dimensions={1}, use_global_device_ids=true | all-gather | bytes 40960 | tf_op jit(solution)/shard_map/all_gather | solution.py:26
  33.8 33.1 %all_gather.23 = bf16[128,2048]{0,1:T(8,128)(2,1)S(1)} all-gather(bf16[128,128]{0,1:T(8,128)(2,1)S(1)} %all_gather.22), channel_id=1, replica_groups=mesh['fs_0'=16,'fs_1'=4,'tp'=8] {'fs_0'}, dimensions={1}, use_global_device_ids=true | all-gather | bytes 557056 | tf_op jit(solution)/shard_map/all_gather | solution.py:26
  66.9 78.5 %all-gather.4.cloned.1.call-done = bf16[2048,256]{1,0:T(8,128)(2,1)} async-done(((bf16[32,256]{1,0:T(8,128)(2,1)}), bf16[2048,256]{1,0:T(8,128)(2,1)}) %all-gather.4.cloned.1.call-update) | async-done | bytes 1048592 | tf_op jit(solution)/shard_map/all_gather | solution.py:20
  145.4 1.5 fusion.30
  150.9 1.5 convolution_convert_fusion.2
  152.5 0.4 convolution_convert_fusion
  152.9 4.3 broadcast_in_dim.4
  157.2 15.8 %all-to-all-start = ((bf16[8,256,2048]{2,1,0:T(8,128)(2,1)}), bf16[8,256,2048]{2,1,0:T(8,128)(2,1)}, u32[]{:S(2)}, u32[]{:S(2)}) async-start(bf16[8,256,2048]{2,1,0:T(8,128)(2,1)} %broadcast_in_dim.4), calls=%async_computation | async-start | bytes 16777216 | tf_op jit(solution)/shard_map/all_to_all | solution.py:32
  173.0 11.0 %all_gather.26 = bf16[1024,128]{0,1:T(8,128)(2,1)} all-gather(bf16[1024,32]{0,1:T(8,128)(2,1)S(1)} %copy-done.2), channel_id=1, replica_groups=mesh['fs_0'=16,'fs_1'=4,'tp'=8] {'fs_1'}, dimensions={1}, use_global_device_ids=true | all-gather | bytes 327680 | tf_op jit(solution)/shard_map/all_gather | solution.py:26
  184.0 82.7 %all-to-all-done = bf16[8,256,2048]{2,1,0:T(8,128)(2,1)} async-done(((bf16[8,256,2048]{2,1,0:T(8,128)(2,1)}), bf16[8,256,2048]{2,1,0:T(8,128)(2,1)}, u32[]{:S(2)}, u32[]{:S(2)}) %all-to-all-start) | async-done | bytes 8388640 | tf_op jit(solution)/shard_map/all_to_all | solution.py:32
  266.7 5.5 %convert_reduce_fusion.1 = f32[256,2048]{1,0:T(8,128)S(1)} fusion(bf16[8,256,2048]{2,1,0:T(8,128)(2,1)} %all-to-all-done), kind=kLoop, calls=%fused_computation.1 | loop fusion | flops 7864320 | bytes 10485760 | tf_op jit(solution)/shard_map/reduce_sum | solution.py:37
  273.1 26.3 %all-gather.8.cloned.1.call-done = bf16[1024,2048]{0,1:T(8,128)(2,1)} async-done(((bf16[1024,128]{0,1:T(8,128)(2,1)}), bf16[1024,2048]{0,1:T(8,128)(2,1)}) %all-gather.8.cloned.1.call-update) | async-done | bytes 4194320 | tf_op jit(solution)/shard_map/all_gather | solution.py:26
  299.4 5.8 %convolution_convert_fusion.1 = bf16[256,2048]{1,0:T(8,128)(2,1)S(1)} fusion(bf16[1024,2048]{0,1:T(8,128)(2,1)} %all-gather.8.cloned.1.call-done, bf16[2048,1024]{1,0:T(8,128)(2,1)} %all-gather.6.cloned.1.call-done, bf16[256,2048]{1,0:T(8,128)(2,1)S(1)} %fusion.3, f32[2048]{0:T(1024)S(1)} %convert_element_type.94, f32[256]{0:T(256)S(1)} %add_rsqrt_fusion.1), kind=kOutput, calls=%fused_computation.9 | convolution fusion | flops 2150891520 | bytes 10494976 | tf_op jit(solution)/shard_map/dot_general | solution.py:146
  305.2 4.3 broadcast_in_dim.5
  309.5 14.4 %all-to-all-start.1 = ((bf16[8,256,2048]{2,1,0:T(8,128)(2,1)}), bf16[8,256,2048]{2,1,0:T(8,128)(2,1)}, u32[]{:S(2)}, u32[]{:S(2)}) async-start(bf16[8,256,2048]{2,1,0:T(8,128)(2,1)} %broadcast_in_dim.5), calls=%async_computation.1 | async-start | bytes 16777216 | tf_op jit(solution)/shard_map/all_to_all | solution.py:32
  324.0 93.7 %all-to-all-done.1 = bf16[8,256,2048]{2,1,0:T(8,128)(2,1)} async-done(((bf16[8,256,2048]{2,1,0:T(8,128)(2,1)}), bf16[8,256,2048]{2,1,0:T(8,128)(2,1)}, u32[]{:S(2)}, u32[]{:S(2)}) %all-to-all-start.1) | async-done | bytes 8388640 | tf_op jit(solution)/shard_map/all_to_all | solution.py:32
  417.7 5.4 %convert_reduce_fusion = f32[256,2048]{1,0:T(8,128)S(1)} fusion(bf16[8,256,2048]{2,1,0:T(8,128)(2,1)} %all-to-all-done.1), kind=kLoop, calls=%fused_computation | loop fusion | flops 7864320 | bytes 10485760 | tf_op jit(solution)/shard_map/reduce_sum | solution.py:37
  423.4 1.4 fusion.7
  (228 shorter events, 4.4 us)
Async XLA Ops:
  6.5 138.8 %copy-start = (bf16[256,2048]{1,0:T(8,128)(2,1)S(1)}, bf16[256,2048]{1,0:T(8,128)(2,1)}, u32[]{:S(2)}) copy-start(bf16[256,2048]{1,0:T(8,128)(2,1)} %param.15) | copy-start | bytes 3145732
  6.5 138.8 %all-gather.4.cloned.1.call-start = ((), (), s32[]{:S(2)}) async-start(), calls=%async_computation.2 | async-start | bytes 1064960 | tf_op jit(solution)/shard_map/all_gather | solution.py:20
  8.0 265.2 %all-gather.6.cloned.1.call-start = ((), (), s32[]{:S(2)}) async-start(), calls=%async_computation.3 | async-start | bytes 4456448 | tf_op jit(solution)/shard_map/all_gather | solution.py:26
  21.4 125.6 %copy-start.6 = (f32[2,256,128]{2,1,0:T(8,128)S(1)}, f32[2,256,128]{2,1,0:T(8,128)}, u32[]{:S(2)}) copy-start(f32[2,256,128]{2,1,0:T(8,128)} %param.23) | copy-start | bytes 786436
  21.4 125.6 %copy-start.7 = (bf16[2,1,128,128]{3,2,1,0:T(8,128)(2,1)S(1)}, bf16[2,1,128,128]{3,2,1,0:T(8,128)(2,1)}, u32[]{:S(2)}) copy-start(bf16[2,1,128,128]{3,2,1,0:T(8,128)(2,1)} %param.20) | copy-start | bytes 196612
  33.8 113.4 %copy-start.8 = (bf16[2,1,128,128]{3,2,1,0:T(8,128)(2,1)S(1)}, bf16[2,1,128,128]{3,2,1,0:T(8,128)(2,1)}, u32[]{:S(2)}) copy-start(bf16[2,1,128,128]{3,2,1,0:T(8,128)(2,1)} %param.21) | copy-start | bytes 196612
  147.4 1.8 copy-start.1
  149.2 0.9 slice-start
  157.2 15.8 %copy-start.2 = (bf16[1024,32]{0,1:T(8,128)(2,1)S(1)}, bf16[1024,32]{0,1:T(8,128)(2,1)}, u32[]{:S(2)}) copy-start(bf16[1024,32]{0,1:T(8,128)(2,1)} %param.28) | copy-start | bytes 196612
  157.2 26.8 %copy-start.3 = (bf16[2048]{0:T(1024)(128)(2,1)S(1)}, bf16[2048]{0:T(1024)(128)(2,1)}, u32[]{:S(2)}) copy-start(bf16[2048]{0:T(1024)(128)(2,1)} %param.25) | copy-start | bytes 12292
  157.2 26.8 %copy-start.4 = (bf16[2048]{0:T(1024)(128)(2,1)S(1)}, bf16[2048]{0:T(1024)(128)(2,1)}, u32[]{:S(2)}) copy-start(bf16[2048]{0:T(1024)(128)(2,1)} %param.26) | copy-start | bytes 12292
  157.2 109.5 %all-to-all-start = ((bf16[8,256,2048]{2,1,0:T(8,128)(2,1)}), bf16[8,256,2048]{2,1,0:T(8,128)(2,1)}, u32[]{:S(2)}, u32[]{:S(2)}) async-start(bf16[8,256,2048]{2,1,0:T(8,128)(2,1)} %broadcast_in_dim.4), calls=%async_computation | async-start | bytes 16777216 | tf_op jit(solution)/shard_map/all_to_all | solution.py:32
  173.0 126.4 %all-gather.8.cloned.1.call-start = ((), (), s32[]{:S(2)}) async-start(), calls=%async_computation.4 | async-start | bytes 4456448 | tf_op jit(solution)/shard_map/all_gather | solution.py:26
  309.5 14.4 %copy-start.5 = (bf16[2048]{0:T(1024)(128)(2,1)S(1)}, bf16[2048]{0:T(1024)(128)(2,1)}, u32[]{:S(2)}) copy-start(bf16[2048]{0:T(1024)(128)(2,1)} %param.29) | copy-start | bytes 12292
  309.5 108.2 %all-to-all-start.1 = ((bf16[8,256,2048]{2,1,0:T(8,128)(2,1)}), bf16[8,256,2048]{2,1,0:T(8,128)(2,1)}, u32[]{:S(2)}, u32[]{:S(2)}) async-start(bf16[8,256,2048]{2,1,0:T(8,128)(2,1)} %broadcast_in_dim.5), calls=%async_computation.1 | async-start | bytes 16777216 | tf_op jit(solution)/shard_map/all_to_all | solution.py:32
Sparse Core Ops, SparseCore 0:
  10.3 135.0 all-gather.3
  147.5 75.4 all-gather.5
  225.1 74.2 all-gather.7
where the time goes:
time: 432 us; the launch traced here: 431 us
  waiting for transfers between devices  281 us (65%)
  blocking collectives  66 us (15%)
  starting transfers between devices  30.2 us (7%)
  other arithmetic  19.2 us (4%)
  between operations  14.2 us (3%)
  local copies, waits for them, and re-layouts  10.3 us (2%)
  matrix products  10.1 us (2%)
    all_to_all x2, waiting for transfers between devices, from_everyone(): return lax.all_to_all(copies, axis, split_axis=0, concat_axis=0, tiled=True)  176 us
    all_gather x1, waiting for transfers between devices, sent_together(): lax.all_gather(both, axis, axis=dim, tiled=True)  78.5 us
    all_gather x4, blocking collectives, gathered_by_axis(): out = lax.all_gather(out, axes[number], axis=dim, tiled=True)  66 us
    all_to_all x2, starting transfers between devices, from_everyone(): return lax.all_to_all(copies, axis, split_axis=0, concat_axis=0, tiled=True)  30.2 us
    all_gather x2, waiting for transfers between devices, gathered_by_axis(): out = lax.all_gather(out, axes[number], axis=dim, tiled=True)  26.3 us
    reduce_sum x2, other arithmetic, taken_together(): return jnp.sum(everything.astype(jnp.float32), axis=0)  10.9 us
  transfers between devices with their start and end apart: 5, of which 4 were waited for; matrix products, arithmetic and copies ran while one was open for 5% of the time, Pallas kernels for 0%

commit v1 on v0

--- a/solution.py
+++ b/solution.py
@@ -4,37 +4,44 @@
 from jax.sharding import Mesh
 from jax.sharding import PartitionSpec as P
 
-FS = ("fs_0", "fs_1")
+FS = ("zh", "zl", "y")
+Z = ("zh", "zl")
+TP = ("x", "c")
 
 
 EPS = 1e-06
 GATE_STEEPNESS = 8.0
 
 
-def sent_together(arrays, axis, dim, along):
-    ends, at = ([], 0)
-    for a in arrays[:-1]:
-        at += a.shape[along]
-        ends.append(at)
-    both = jnp.concatenate(arrays, axis=along)
-    return tuple(jnp.split(lax.all_gather(both, axis, axis=dim, tiled=True), ends, axis=along))
-
-
-def gathered_by_axis(array, axes, dim):
-    out = array
-    for number in range(len(axes) - 1, -1, -1):
-        out = lax.all_gather(out, axes[number], axis=dim, tiled=True)
-    return out
-
-
-def from_everyone(array, axis):
+def spread(array, axis):
     copies = jnp.broadcast_to(array, (lax.axis_size(axis), *array.shape))
     return lax.all_to_all(copies, axis, split_axis=0, concat_axis=0, tiled=True)
 
 
-def taken_together(array, axis):
-    everything = from_everyone(array, axis)
-    return jnp.sum(everything.astype(jnp.float32), axis=0)
+def mixer_weights(array):
+    width = array.shape[-1]
+    pieces = spread(spread(spread(array, "zh"), "zl"), "y")
+    return jnp.transpose(pieces, (2, 1, 0, 3, 4)).reshape(-1, width)
+
+
+def feedforward_weights(array):
+    near = spread(array, "y").reshape(-1, array.shape[-1])
+    return lax.all_gather(near, Z, axis=0, tiled=True)
+
+
+def summed_rows(partial):
+    cores, wide = lax.axis_size("c"), lax.axis_size("x")
+    rows, width = partial.shape
+    halves = partial.astype(jnp.bfloat16).reshape(cores, rows // cores, width)
+    pair = lax.all_to_all(halves, "c", split_axis=0, concat_axis=0, tiled=True)
+    half = jnp.sum(pair.astype(jnp.float32), axis=0).astype(jnp.bfloat16)
+    quarters = half.reshape(wide, rows // (cores * wide), width)
+    several = lax.all_to_all(quarters, "x", split_axis=0, concat_axis=0, tiled=True)
+    return jnp.sum(several.astype(jnp.float32), axis=0)
+
+
+def all_rows(part):
+    return spread(spread(part, "x"), "c").reshape(-1, part.shape[-1])
 
 
 def root_norm(values, gain):
@@ -103,11 +110,21 @@
     feedforward_down_weight,
     feedforward_output_gain,
 ):
+    mixer = mixer_weights(
+        jnp.concatenate(
+            (recurrent_branch_weight, output_gate_weight, recurrent_output_weight.T), axis=1
+        )
+    )
+    forward = feedforward_weights(
+        jnp.concatenate((feedforward_up_weight, feedforward_down_weight.T), axis=1)
+    )
+    channels = recurrent_branch_weight.shape[1]
+    hidden_units = feedforward_up_weight.shape[1]
     normed = root_norm(tokens.astype(jnp.float32), recurrent_input_gain).astype(jnp.bfloat16)
-    pieces = sent_together((recurrent_branch_weight, output_gate_weight), FS, 0, 1)
-    columns = normed
-    recur_sum = jnp.dot(columns, pieces[0], preferred_element_type=jnp.float32)
-    gate_sum = jnp.dot(columns, pieces[1], preferred_element_type=jnp.float32)
+    recur_sum = jnp.dot(normed, mixer[:, :channels], preferred_element_type=jnp.float32)
+    gate_sum = jnp.dot(
+        normed, mixer[:, channels : 2 * channels], preferred_element_type=jnp.float32
+    )
     recur_in = recur_sum.astype(jnp.bfloat16)
     gate_in = lax.optimization_barrier(gate_sum.astype(jnp.bfloat16))
     convolved_output = lax.optimization_barrier(centred_conv(recur_in, filter_taps))
@@ -130,43 +147,50 @@
     hidden = ((forward_sweep + backward_sweep) * jax.nn.gelu(gate_in.astype(jnp.float32))).astype(
         jnp.bfloat16
     )
-    mixer_cols = gathered_by_axis(recurrent_output_weight, FS, 1)
-    partial_value = jnp.dot(hidden, mixer_cols, preferred_element_type=jnp.float32)
-    mixed = taken_together(partial_value.astype(jnp.bfloat16), "tp").astype(jnp.float32)
+    across = (((1,), (1,)), ((), ()))
+    partial_value = lax.dot_general(
+        hidden, mixer[:, 2 * channels :], across, preferred_element_type=jnp.float32
+    )
+    mixed = summed_rows(partial_value)
+    share = mixed.shape[0]
+    place = lax.axis_index("c") * lax.axis_size("x") + lax.axis_index("x")
+    own = lax.dynamic_slice_in_dim(tokens, place * share, share, axis=0)
     stream = lax.optimization_barrier(
-        (tokens.astype(jnp.float32) + root_norm(mixed, recurrent_output_gain)).astype(jnp.bfloat16)
+        (own.astype(jnp.float32) + root_norm(mixed, recurrent_output_gain)).astype(jnp.bfloat16)
     )
-    normed_ff = root_norm(stream.astype(jnp.float32), feedforward_norm_gain).astype(jnp.bfloat16)
-    columns = normed_ff
-    lifted_sum = jnp.dot(
-        columns, gathered_by_axis(feedforward_up_weight, FS, 0), preferred_element_type=jnp.float32
+    normed_ff = all_rows(
+        root_norm(stream.astype(jnp.float32), feedforward_norm_gain).astype(jnp.bfloat16)
     )
+    lifted_sum = jnp.dot(normed_ff, forward[:, :hidden_units], preferred_element_type=jnp.float32)
     lifted = jnp.square(jax.nn.relu(lifted_sum)).astype(jnp.bfloat16)
-    down_cols = gathered_by_axis(feedforward_down_weight, FS, 1)
-    lowered_part = jnp.dot(lifted, down_cols, preferred_element_type=jnp.float32)
-    lowered = taken_together(lowered_part.astype(jnp.bfloat16), "tp").astype(jnp.float32)
-    return (stream.astype(jnp.float32) + root_norm(lowered, feedforward_output_gain)).astype(
-        jnp.bfloat16
+    lowered_part = lax.dot_general(
+        lifted, forward[:, hidden_units:], across, preferred_element_type=jnp.float32
+    )
+    lowered = summed_rows(lowered_part)
+    return all_rows(
+        (stream.astype(jnp.float32) + root_norm(lowered, feedforward_output_gain)).astype(
+            jnp.bfloat16
+        )
     )
 
 
 def solution(mesh):
-    split = Mesh(mesh.devices.reshape(16, 4, mesh.shape["tp"]), ("fs_0", "fs_1", "tp"))
+    split = Mesh(mesh.devices.reshape(4, 4, 4, 4, 2), ("zh", "zl", "y", "x", "c"))
     placed = (
         P(FS, None),
         P(),
-        P(FS, "tp"),
-        P(FS, "tp"),
-        P(None, "tp"),
-        P(None, "tp", None, None),
-        P(None, "tp", None, None),
-        P(None, "tp"),
-        P(None, FS, "tp"),
-        P("tp", FS),
+        P(FS, TP),
+        P(FS, TP),
+        P(None, TP),
+        P(None, TP, None, None),
+        P(None, TP, None, None),
+        P(None, TP),
+        P(None, FS, TP),
+        P(TP, FS),
         P(),
         P(),
-        P(FS, "tp"),
-        P("tp", FS),
+        P(FS, TP),
+        P(TP, FS),
         P(),
     )
     return jax.shard_map(

time: 432 us -> 199 us (0.46)
  waiting for transfers between devices: 281 us -> 64.2 us
  other arithmetic: 19.2 us -> 5.67 us
    all_to_all x2 -> x5, waiting for transfers between devices: 176 us -> 47.4 us  [the longest x3 29.5 us: spread(): return lax.all_to_all(copies, axis, split_axis=0, concat_axis=0, tiled=True)]
    all_gather x3 -> x1, waiting for transfers between devices: 105 us -> 16.2 us  [feedforward_weights(): return lax.all_gather(near, Z, axis=0, tiled=True)]
    all_gather x4 -> x0, blocking collectives: 66 us -> none  [gathered_by_axis(): out = lax.all_gather(out, axes[number], axis=dim, tiled=True)]
    all_to_all x0 -> x7, blocking collectives: none -> 64.5 us  [the longest x5 44.6 us: spread(): return lax.all_to_all(copies, axis, split_axis=0, concat_axis=0, tiled=True)]
    reduce_sum x2 -> x4, other arithmetic: 10.9 us -> 2.39 us  [the longest x2 2.23 us: summed_rows(): half = jnp.sum(pair.astype(jnp.float32), axis=0).astype(jnp.bfloat16)]
    broadcast_in_dim x2 -> x8, local copies, waits for them, and re-layouts: 8.56 us -> 3.31 us  [spread(): copies = jnp.broadcast_to(array, (lax.axis_size(axis), *array.shape))]
    all_to_all x2 -> x5, starting transfers between devices: 30.2 us -> 32.8 us  [the longest x3 24.9 us: spread(): return lax.all_to_all(copies, axis, split_axis=0, concat_axis=0, tiled=True)]
  transfers between devices with their start and end apart: 5 -> 6, of which waited for: 4 -> 6; matrix products, arithmetic and copies ran while one was open for 5% -> 5% of each run, Pallas kernels for 0% -> 0%
where the time goes in v1:
time: 199 us; the launch traced here: 198 us
  blocking collectives  64.5 us (32%)
  waiting for transfers between devices  64.2 us (32%)
  starting transfers between devices  32.8 us (16%)
  between operations  14.6 us (7%)
  matrix products  9.29 us (5%)
  local copies, waits for them, and re-layouts  6.69 us (3%)
  other arithmetic  5.67 us (3%)
    all_to_all x5, blocking collectives, spread(): return lax.all_to_all(copies, axis, split_axis=0, concat_axis=0, tiled=True)  44.6 us
    all_to_all x3, waiting for transfers between devices, spread(): return lax.all_to_all(copies, axis, split_axis=0, concat_axis=0, tiled=True)  29.5 us
    all_to_all x3, starting transfers between devices, spread(): return lax.all_to_all(copies, axis, split_axis=0, concat_axis=0, tiled=True)  24.9 us
    all_to_all x2, blocking collectives, summed_rows(): pair = lax.all_to_all(halves, 'c', split_axis=0, concat_axis=0, tiled=True)  19.9 us
    all_to_all x2, waiting for transfers between devices, summed_rows(): lax.all_to_all(quarters, 'x', split_axis=0, concat_axis=0, tiled=True)  17.8 us
    all_gather x1, waiting for transfers between devices, feedforward_weights(): return lax.all_gather(near, Z, axis=0, tiled=True)  16.2 us
    all_to_all x2, starting transfers between devices, summed_rows(): lax.all_to_all(quarters, 'x', split_axis=0, concat_axis=0, tiled=True)  7.93 us
    dot_general x1, matrix products, per_device(): lax.dot_general(lifted, forward[:, hidden_units:], across, preferred_elem...  5.81 us
  transfers between devices with their start and end apart: 6, of which 6 were waited for; matrix products, arithmetic and copies ran while one was open for 5% of the time, Pallas kernels for 0%

profile of v1, /device:TPU:1, one launch (start us, length us, event | category | flops | bytes accessed | tf_op | source)
XLA Modules:
  0.0 197.8 jit_solution(3775342261377524410)
XLA Ops:
  8.3 5.0 %all-to-all-start.7 = ((bf16[4,32,2048]{2,1,0:T(8,128)(2,1)}), bf16[4,32,2048]{2,1,0:T(8,128)(2,1)S(1)}, u32[]{:S(2)}, u32[]{:S(2)}) async-start(bf16[4,32,2048]{2,1,0:T(8,128)(2,1)} %broadcast_in_dim.41), calls=%async_computation.7 | async-start | bytes 1048576 | tf_op jit(solution)/shard_map/all_to_all | solution.py:18
  14.0 6.2 %all-to-all-done.7 = bf16[4,32,2048]{2,1,0:T(8,128)(2,1)S(1)} async-done(((bf16[4,32,2048]{2,1,0:T(8,128)(2,1)}), bf16[4,32,2048]{2,1,0:T(8,128)(2,1)S(1)}, u32[]{:S(2)}, u32[]{:S(2)}) %all-to-all-start.7) | async-done | bytes 524320 | tf_op jit(solution)/shard_map/all_to_all | solution.py:18
  20.9 16.2 %all-to-all-start = ((bf16[4,32,384]{2,1,0:T(8,128)(2,1)}), bf16[4,32,384]{2,1,0:T(8,128)(2,1)S(1)}, u32[]{:S(2)}, u32[]{:S(2)}) async-start(bf16[4,32,384]{2,1,0:T(8,128)(2,1)} %broadcast_in_dim.16), calls=%async_computation | async-start | bytes 196608 | tf_op jit(solution)/shard_map/all_to_all | solution.py:18
  37.8 11.2 %all-to-all-done = bf16[4,32,384]{2,1,0:T(8,128)(2,1)S(1)} async-done(((bf16[4,32,384]{2,1,0:T(8,128)(2,1)}), bf16[4,32,384]{2,1,0:T(8,128)(2,1)S(1)}, u32[]{:S(2)}, u32[]{:S(2)}) %all-to-all-start) | async-done | bytes 98336 | tf_op jit(solution)/shard_map/all_to_all | solution.py:18
  49.0 10.6 %all_to_all.60 = bf16[4,4,32,384]{3,2,1,0:T(8,128)(2,1)S(1)} all-to-all(bf16[4,4,32,384]{3,2,1,0:T(8,128)(2,1)S(1)} %broadcast_in_dim.17), channel_id=1, replica_groups=mesh['zh'=4,'zl'=4,'y'=4,'x'=4,'c'=2] {'zl'}, dimensions={0} | all-to-all | bytes 786432 | tf_op jit(solution)/shard_map/all_to_all | solution.py:18
  59.6 1.4 broadcast_in_dim.18
  61.1 3.7 %all-to-all-start.2 = ((bf16[4,4,4,32,384]{4,3,1,2,0:T(8,128)(2,1)}), bf16[4,4,4,32,384]{4,3,1,2,0:T(8,128)(2,1)S(1)}, u32[]{:S(2)}, u32[]{:S(2)}) async-start(bf16[4,4,4,32,384]{4,3,1,2,0:T(8,128)(2,1)} %broadcast_in_dim.18), calls=%async_computation.2 | async-start | bytes 3145728 | tf_op jit(solution)/shard_map/all_to_all | solution.py:18
  65.1 12.2 %all-to-all-done.2 = bf16[4,4,4,32,384]{4,3,1,2,0:T(8,128)(2,1)S(1)} async-done(((bf16[4,4,4,32,384]{4,3,1,2,0:T(8,128)(2,1)}), bf16[4,4,4,32,384]{4,3,1,2,0:T(8,128)(2,1)S(1)}, u32[]{:S(2)}, u32[]{:S(2)}) %all-to-all-start.2) | async-done | bytes 1572896 | tf_op jit(solution)/shard_map/all_to_all | solution.py:18
  77.6 1.8 fusion.41
  84.7 14.9 %all_to_all.61 = bf16[2,128,2048]{2,1,0:T(8,128)(2,1)S(1)} all-to-all(bf16[2,128,2048]{2,1,0:T(8,128)(2,1)S(1)} %bitcast.53), channel_id=1, replica_groups=mesh['zh'=4,'zl'=4,'y'=4,'x'=4,'c'=2] {'c'}, dimensions={0} | all-to-all | bytes 2097152 | tf_op jit(solution)/shard_map/all_to_all | solution.py:36
  99.7 1.1 reduce_sum.79
  100.8 4.0 %all-to-all-start.4 = ((bf16[4,32,2048]{2,1,0:T(8,128)(2,1)}), bf16[4,32,2048]{2,1,0:T(8,128)(2,1)S(1)}, u32[]{:S(2)}, u32[]{:S(2)}) async-start(bf16[4,32,2048]{2,1,0:T(8,128)(2,1)} %bitcast.17), calls=%async_computation.4 | async-start | bytes 1048576 | tf_op jit(solution)/shard_map/all_to_all | solution.py:39
  104.8 8.9 %all-to-all-done.4 = bf16[4,32,2048]{2,1,0:T(8,128)(2,1)S(1)} async-done(((bf16[4,32,2048]{2,1,0:T(8,128)(2,1)}), bf16[4,32,2048]{2,1,0:T(8,128)(2,1)S(1)}, u32[]{:S(2)}, u32[]{:S(2)}) %all-to-all-start.4) | async-done | bytes 524320 | tf_op jit(solution)/shard_map/all_to_all | solution.py:39
  114.3 10.2 %all_to_all.62 = bf16[4,32,2048]{2,1,0:T(8,128)(2,1)S(1)} all-to-all(bf16[4,32,2048]{2,1,0:T(8,128)(2,1)S(1)} %broadcast_in_dim.19), channel_id=1, replica_groups=mesh['zh'=4,'zl'=4,'y'=4,'x'=4,'c'=2] {'x'}, dimensions={0} | all-to-all | bytes 1048576 | tf_op jit(solution)/shard_map/all_to_all | solution.py:18
  124.7 6.8 %all_to_all.63 = bf16[2,4,32,2048]{3,2,1,0:T(8,128)(2,1)S(1)} all-to-all(bf16[2,4,32,2048]{3,2,1,0:T(8,128)(2,1)S(1)} %broadcast_in_dim.40), channel_id=1, replica_groups=mesh['zh'=4,'zl'=4,'y'=4,'x'=4,'c'=2] {'c'}, dimensions={0} | all-to-all | bytes 2097152 | tf_op jit(solution)/shard_map/all_to_all | solution.py:18
  131.5 16.2 %all-gather.2.cloned.1.call-done = bf16[2048,2048]{1,0:T(8,128)(2,1)} async-done(((bf16[128,2048]{1,0:T(8,128)(2,1)}), bf16[2048,2048]{1,0:T(8,128)(2,1)}) %all-gather.2.cloned.1.call-update) | async-done | bytes 8388624 | tf_op jit(solution)/shard_map/all_gather | solution.py:29
  147.7 5.8 %fusion.4 = bf16[256,2048]{1,0:T(8,128)(2,1)S(1)} fusion(bf16[2048,2048]{1,0:T(8,128)(2,1)} %all-gather.2.cloned.1.call-done, bf16[256,2048]{1,0:T(8,128)(2,1)S(1)} %bitcast.59), kind=kOutput, calls=%fused_computation.7 | convolution fusion | flops 2148794368 | bytes 10485760 | tf_op jit(solution)/shard_map/dot_general | solution.py:166
  153.5 5.0 %all_to_all.64 = bf16[2,128,2048]{2,1,0:T(8,128)(2,1)S(1)} all-to-all(bf16[2,128,2048]{2,1,0:T(8,128)(2,1)S(1)} %bitcast.60), channel_id=1, replica_groups=mesh['zh'=4,'zl'=4,'y'=4,'x'=4,'c'=2] {'c'}, dimensions={0} | all-to-all | bytes 2097152 | tf_op jit(solution)/shard_map/all_to_all | solution.py:36
  158.5 1.1 reduce_sum.83
  159.6 4.0 %all-to-all-start.9 = ((bf16[4,32,2048]{2,1,0:T(8,128)(2,1)}), bf16[4,32,2048]{2,1,0:T(8,128)(2,1)S(1)}, u32[]{:S(2)}, u32[]{:S(2)}) async-start(bf16[4,32,2048]{2,1,0:T(8,128)(2,1)} %bitcast.22), calls=%async_computation.9 | async-start | bytes 1048576 | tf_op jit(solution)/shard_map/all_to_all | solution.py:39
  163.5 8.9 %all-to-all-done.9 = bf16[4,32,2048]{2,1,0:T(8,128)(2,1)S(1)} async-done(((bf16[4,32,2048]{2,1,0:T(8,128)(2,1)}), bf16[4,32,2048]{2,1,0:T(8,128)(2,1)S(1)}, u32[]{:S(2)}, u32[]{:S(2)}) %all-to-all-start.9) | async-done | bytes 524320 | tf_op jit(solution)/shard_map/all_to_all | solution.py:39
  172.8 10.2 %all_to_all.65 = bf16[4,32,2048]{2,1,0:T(8,128)(2,1)S(1)} all-to-all(bf16[4,32,2048]{2,1,0:T(8,128)(2,1)S(1)} %broadcast_in_dim.42), channel_id=1, replica_groups=mesh['zh'=4,'zl'=4,'y'=4,'x'=4,'c'=2] {'x'}, dimensions={0} | all-to-all | bytes 1048576 | tf_op jit(solution)/shard_map/all_to_all | solution.py:18
  183.2 6.8 %all_to_all.66 = bf16[2,4,32,2048]{3,2,1,0:T(8,128)(2,1)S(1)} all-to-all(bf16[2,4,32,2048]{3,2,1,0:T(8,128)(2,1)S(1)} %broadcast_in_dim.43), channel_id=1, replica_groups=mesh['zh'=4,'zl'=4,'y'=4,'x'=4,'c'=2] {'c'}, dimensions={0} | all-to-all | bytes 2097152 | tf_op jit(solution)/shard_map/all_to_all | solution.py:18
  190.0 1.0 copy.21
  (252 shorter events, 10.2 us)
Async XLA Ops:
  8.3 11.9 %all-to-all-start.7 = ((bf16[4,32,2048]{2,1,0:T(8,128)(2,1)}), bf16[4,32,2048]{2,1,0:T(8,128)(2,1)S(1)}, u32[]{:S(2)}, u32[]{:S(2)}) async-start(bf16[4,32,2048]{2,1,0:T(8,128)(2,1)} %broadcast_in_dim.41), calls=%async_computation.7 | async-start | bytes 1048576 | tf_op jit(solution)/shard_map/all_to_all | solution.py:18
  20.2 16.9 %copy-start = (bf16[4,32,2048]{2,1,0:T(8,128)(2,1)}, bf16[4,32,2048]{2,1,0:T(8,128)(2,1)S(1)}, u32[]{:S(2)}) copy-start(bf16[4,32,2048]{2,1,0:T(8,128)(2,1)S(1)} %all-to-all-done.7) | copy-start | bytes 1572868
  20.9 28.1 %all-to-all-start = ((bf16[4,32,384]{2,1,0:T(8,128)(2,1)}), bf16[4,32,384]{2,1,0:T(8,128)(2,1)S(1)}, u32[]{:S(2)}, u32[]{:S(2)}) async-start(bf16[4,32,384]{2,1,0:T(8,128)(2,1)} %broadcast_in_dim.16), calls=%async_computation | async-start | bytes 196608 | tf_op jit(solution)/shard_map/all_to_all | solution.py:18
  37.1 110.6 %all-gather.2.cloned.1.call-start = ((), (), s32[]{:S(2)}) async-start(), calls=%async_computation.12 | async-start | bytes 8912896 | tf_op jit(solution)/shard_map/all_gather | solution.py:29
  59.6 5.1 %copy-start.4 = (bf16[2048]{0:T(1024)(128)(2,1)S(1)}, bf16[2048]{0:T(1024)(128)(2,1)}, u32[]{:S(2)}) copy-start(bf16[2048]{0:T(1024)(128)(2,1)} %param.16) | copy-start | bytes 12292
  61.0 3.7 %copy-start.1 = (bf16[256,2048]{1,0:T(8,128)(2,1)S(1)}, bf16[256,2048]{1,0:T(8,128)(2,1)}, u32[]{:S(2)}) copy-start(bf16[256,2048]{1,0:T(8,128)(2,1)} %param.15) | copy-start | bytes 3145732
  61.0 4.0 %copy-start.9 = (f32[2,128]{1,0:T(2,128)S(1)}, f32[2,128]{1,0:T(2,128)}, u32[]{:S(2)}) copy-start(f32[2,128]{1,0:T(2,128)} %param.22) | copy-start | bytes 3076
  61.0 4.1 %copy-start.8 = (bf16[4,128]{1,0:T(4,128)(2,1)S(1)}, bf16[4,128]{1,0:T(4,128)(2,1)}, u32[]{:S(2)}) copy-start(bf16[4,128]{1,0:T(4,128)(2,1)} %param.19) | copy-start | bytes 3076
  61.1 16.3 %all-to-all-start.2 = ((bf16[4,4,4,32,384]{4,3,1,2,0:T(8,128)(2,1)}), bf16[4,4,4,32,384]{4,3,1,2,0:T(8,128)(2,1)S(1)}, u32[]{:S(2)}, u32[]{:S(2)}) async-start(bf16[4,4,4,32,384]{4,3,1,2,0:T(8,128)(2,1)} %broadcast_in_dim.18), calls=%async_computation.2 | async-start | bytes 3145728 | tf_op jit(solution)/shard_map/all_to_all | solution.py:18
  77.6 1.9 copy-start.10
  77.6 1.9 copy-start.11
  77.6 2.1 %copy-start.12 = (bf16[2,1,128,128]{3,2,1,0:T(8,128)(2,1)S(1)}, bf16[2,1,128,128]{3,2,1,0:T(8,128)(2,1)}, u32[]{:S(2)}) copy-start(bf16[2,1,128,128]{3,2,1,0:T(8,128)(2,1)} %param.21) | copy-start | bytes 196612
  79.9 1.3 copy-start.3
  81.3 1.4 slice-start
  82.5 1.2 copy-start.2
  84.7 20.0 %copy-start.5 = (bf16[2048]{0:T(1024)(128)(2,1)S(1)}, bf16[2048]{0:T(1024)(128)(2,1)}, u32[]{:S(2)}) copy-start(bf16[2048]{0:T(1024)(128)(2,1)} %param.25) | copy-start | bytes 12292
  84.7 20.0 %copy-start.6 = (bf16[2048]{0:T(1024)(128)(2,1)S(1)}, bf16[2048]{0:T(1024)(128)(2,1)}, u32[]{:S(2)}) copy-start(bf16[2048]{0:T(1024)(128)(2,1)} %param.26) | copy-start | bytes 12292
  100.8 12.9 %all-to-all-start.4 = ((bf16[4,32,2048]{2,1,0:T(8,128)(2,1)}), bf16[4,32,2048]{2,1,0:T(8,128)(2,1)S(1)}, u32[]{:S(2)}, u32[]{:S(2)}) async-start(bf16[4,32,2048]{2,1,0:T(8,128)(2,1)} %bitcast.17), calls=%async_computation.4 | async-start | bytes 1048576 | tf_op jit(solution)/shard_map/all_to_all | solution.py:39
  153.5 10.1 %copy-start.7 = (bf16[2048]{0:T(1024)(128)(2,1)S(1)}, bf16[2048]{0:T(1024)(128)(2,1)}, u32[]{:S(2)}) copy-start(bf16[2048]{0:T(1024)(128)(2,1)} %param.29) | copy-start | bytes 12292
  159.6 12.9 %all-to-all-start.9 = ((bf16[4,32,2048]{2,1,0:T(8,128)(2,1)}), bf16[4,32,2048]{2,1,0:T(8,128)(2,1)S(1)}, u32[]{:S(2)}, u32[]{:S(2)}) async-start(bf16[4,32,2048]{2,1,0:T(8,128)(2,1)} %bitcast.22), calls=%async_computation.9 | async-start | bytes 1048576 | tf_op jit(solution)/shard_map/all_to_all | solution.py:39
Sparse Core Ops, SparseCore 0:
  40.0 107.6 all-gather.1
